TPU v7x, 32 devices: a whole 2x2x4 slice. The times are simulated.
32 devices in a mesh: sp: 4 (over z), fs: 4 (over y, x), tp: 2 (over core).
Axes of the slice: x: 2, y: 2, z: 4, core: 2. Of those that a mesh axis runs over, the one named last changes fastest.
Arguments:
- tokens: bfloat16 [2048, 2048], P(('fs', 'sp')), may hold values from -6 to 6
- in_gain: float32 [2048], replicated, may hold values from 0.1 to 1.9
- query_weight: bfloat16 [2048, 512], P(None, ('tp', 'fs')), may hold values from -0.17291713 to 0.17291713
- key_weight: bfloat16 [2048, 512], P(None, ('tp', 'fs')), may hold values from -0.17291713 to 0.17291713
- value_weight: bfloat16 [2048, 512], P(None, ('tp', 'fs')), may hold values from -0.125 to 0.125
- rec_query_weight: bfloat16 [2048, 512], P(None, ('tp', 'fs')), may hold values from -0.125 to 0.125
- rec_forget_weight: bfloat16 [2048, 512], P(None, ('tp', 'fs')), may hold values from -0.125 to 0.125
- rec_input_weight: bfloat16 [2048, 512], P(None, ('tp', 'fs')), may hold values from -0.125 to 0.125
- mix_lambda: float32 [4], P('tp'), may hold values from 0.3 to 0.8
- lower_bound: float32 [4, 128], P('tp'), may hold values from 0.9 to 0.9995117
- forget_scale: float32 [2048], P(('fs', 'sp')), may hold values from 0.35 to 1536
- att_gain: float32 [128], replicated, may hold values from 0.1 to 1.9
- recurrence_gain: float32 [128], replicated, may hold values from 0.1 to 1.9
- att_out_weight: bfloat16 [512, 2048], P('tp'), may hold values from -0.1875 to 0.1875
- rec_out_weight: bfloat16 [512, 2048], P('tp'), may hold values from -0.1875 to 0.1875
Outputs:
- mixed_out: bfloat16 [2048, 2048], P(('fs', 'sp'))
- log_weight_sum: float32 [4, 2048], P('tp', ('fs', 'sp'))
All inputs are finite; a program needn't handle non-finite values.
Results may differ from a plain program's by a relative error of at most 0.012.
Values may be sent and summed in bfloat16 or wider, within the bound.
A program may use at most 128 MiB of HBM per device.

v0:
```python
import jax
import jax.numpy as jnp
from jax import lax
from jax.sharding import PartitionSpec as P

DK = 64
DV = 128
BLK = 64
EPS = 1e-06
NEG = -1e30


def from_behind(value, axis, steps):
    count = lax.axis_size(axis)
    initial, last = (max(0, -steps), min(count, count - steps))
    return lax.ppermute(value, axis, [(source, source + steps) for source in range(initial, last)])


def entering(value, axis, join, neutral):
    count, mine = (lax.axis_size(axis), lax.axis_index(axis))
    pieces = jax.tree.map(lambda part: lax.all_gather(part, axis), value)
    running = jax.tree.map(
        lambda part, zero: jnp.full_like(part, 0) + jnp.asarray(zero, part.dtype), value, neutral
    )

    def step(position, running):
        longer = join(running, jax.tree.map(lambda part: part[position], pieces))
        return jax.tree.map(lambda new, old: jnp.where(position < mine, new, old), longer, running)

    return lax.fori_loop(0, count - 1, step, running)


def norm_rows(values, gain):
    return values * lax.rsqrt(jnp.mean(values * values, axis=-1, keepdims=True) + EPS) * gain


def block_recurrence(queries, key_in, value_in, log_forget):
    head_count, row_count, key_width = queries.shape
    block_count = row_count // BLK

    def to_blocks(array_in):
        return array_in.reshape(head_count, block_count, BLK, array_in.shape[-1]).transpose(
            1, 0, 2, 3
        )

    causal = jnp.tril(jnp.ones((BLK, BLK), bool))

    def advance(passed_state, inputs):
        query_block, key_block, value_block, l_blk = inputs
        accumulator_sum = jnp.cumsum(l_blk, axis=1)
        cross_block_output = jnp.einsum(
            "sre,sei->sri",
            query_block * jnp.exp(accumulator_sum),
            passed_state,
            precision=lax.Precision.HIGHEST,
        )
        spread = accumulator_sum[:, :, None, :] - accumulator_sum[:, None, :, :]
        decay = jnp.exp(jnp.where(causal[None, :, :, None], spread, -jnp.inf))
        scores = jnp.einsum(
            "htk,htsk,hsk->hts", query_block, decay, key_block, precision=lax.Precision.HIGHEST
        )
        result = cross_block_output + jnp.einsum(
            "hts,hsv->htv", scores, value_block, precision=lax.Precision.HIGHEST
        )
        final_log_sum = accumulator_sum[:, -1:, :]
        updated_state = jnp.exp(final_log_sum[:, 0, :])[:, :, None] * passed_state + jnp.einsum(
            "plf,plt->pft",
            key_block * jnp.exp(final_log_sum - accumulator_sum),
            value_block,
            precision=lax.Precision.HIGHEST,
        )
        return (updated_state, result)

    begin_state = jnp.zeros((head_count, key_width, value_in.shape[-1]), jnp.float32)
    end_state, results = lax.scan(
        advance,
        begin_state,
        (to_blocks(queries), to_blocks(key_in), to_blocks(value_in), to_blocks(log_forget)),
    )
    return (
        end_state,
        results.transpose(1, 0, 2, 3).reshape(head_count, row_count, value_in.shape[-1]),
    )


def attend(online, queries, pair_keys, pair_values, allowed):
    running_max, weight_sum, numer_sum = online
    local_heads = numer_sum.shape[0]
    key_rows = pair_keys.shape[0]
    key_heads = pair_keys.reshape(key_rows, local_heads, 2, DK).transpose(1, 2, 0, 3)
    head_values = pair_values.reshape(key_rows, local_heads, DV).transpose(1, 0, 2)
    scores = jnp.einsum(
        "hmqd,hmkd->hmqk", queries, key_heads, preferred_element_type=jnp.float32
    ) * DK ** (-0.5)
    scores = jnp.where(allowed, scores, NEG)
    highest = jnp.maximum(running_max, jnp.max(scores, axis=-1))
    weights = jnp.exp(scores - highest[..., None])
    shrink = jnp.exp(running_max - highest)
    weight_sum = weight_sum * shrink + jnp.sum(weights, axis=-1)
    numer_sum = numer_sum * shrink[..., None] + jnp.einsum(
        "itap,ipn->itan",
        weights.astype(jnp.bfloat16),
        head_values,
        preferred_element_type=jnp.float32,
    )
    return (highest, weight_sum, numer_sum)


def attend_pieces(online, queries, pieces, first_offset, position):

    def visit(piece_index, inner):
        piece = lax.dynamic_index_in_dim(pieces, piece_index, 0, keepdims=False)
        return lax.cond(
            position >= first_offset + piece_index,
            lambda state: attend(state, queries, piece[0], piece[1], True),
            lambda state: state,
            inner,
        )

    return lax.fori_loop(0, pieces.shape[0], visit, online)


def on_device(
    tokens,
    in_gain,
    query_weight,
    key_weight,
    value_weight,
    rec_query_weight,
    rec_forget_weight,
    rec_input_weight,
    mix_lambda,
    lower_bound,
    forget_scale,
    att_gain,
    recurrence_gain,
    att_out_weight,
    rec_out_weight,
):
    normed = norm_rows(tokens.astype(jnp.float32), in_gain).astype(jnp.bfloat16)
    row_count = normed.shape[0]
    stacked = jnp.stack(
        [
            query_weight,
            key_weight,
            value_weight,
            rec_query_weight,
            rec_forget_weight,
            rec_input_weight,
        ],
        axis=1,
    )
    projected = jnp.einsum(
        "rd,dnc->rnc",
        normed,
        lax.all_gather(stacked, "fs", axis=2, tiled=True),
        preferred_element_type=jnp.float32,
    ).astype(jnp.bfloat16)
    local_heads = projected.shape[2] // DV
    position = lax.axis_index("sp")
    queries = projected[:, 0].reshape(row_count, local_heads, 2, DK).transpose(1, 2, 0, 3)
    online = (
        jnp.full((local_heads, 2, row_count), NEG, jnp.float32),
        jnp.zeros((local_heads, 2, row_count), jnp.float32),
        jnp.zeros((local_heads, 2, row_count, DV), jnp.float32),
    )
    moving = jnp.stack([projected[:, 1], projected[:, 2]])
    causal = jnp.arange(row_count)[:, None] >= jnp.arange(row_count)[None, :]
    online = attend(online, queries, moving[0], moving[1], causal)
    buffer = moving[None]
    levels = (lax.axis_size("sp") - 1).bit_length()
    offset_now = 1
    for level_index in range(levels):
        received = from_behind(buffer, "sp", offset_now)
        online = attend_pieces(online, queries, received, offset_now, position)
        if level_index + 1 < levels:
            buffer = jnp.concatenate([buffer, received], axis=0)
        offset_now = offset_now * 2
    running_max, weight_sum, numer_sum = online
    mixed_heads = (
        numer_sum[:, 0] / weight_sum[:, 0, :, None]
        - mix_lambda[:, None, None] * numer_sum[:, 1] / weight_sum[:, 1, :, None]
    )
    att_heads = (norm_rows(mixed_heads, att_gain) * 0.8).astype(jnp.bfloat16)
    att_rows = att_heads.transpose(1, 0, 2).reshape(row_count, local_heads * DV)
    log_weight_sum = running_max[:, 0] + jnp.log(weight_sum[:, 0])

    def heads_first(array_in):
        return array_in.reshape(row_count, local_heads, DV).transpose(1, 0, 2).astype(jnp.float32)

    recurrent_queries = heads_first(projected[:, 3])
    lower_edge = lower_bound[:, None, :]
    forget = lower_edge + (1.0 - lower_edge) * jax.nn.sigmoid(heads_first(projected[:, 4]))
    log_forget = forget_scale[None, :, None] * jnp.log(forget)
    key_in = 1.0 - jnp.exp(log_forget)
    end_state, local_result = block_recurrence(
        recurrent_queries, key_in, heads_first(projected[:, 5]), log_forget
    )
    running_state = jnp.cumsum(log_forget, axis=1)
    carry_rate = jnp.exp(running_state[:, -1, :])

    def combine(earlier, later):
        return (later[0] * earlier[0], later[0][..., None] * earlier[1] + later[1])

    identity = (jnp.ones_like(carry_rate), jnp.zeros_like(end_state))
    _, incoming_state = entering((carry_rate, end_state), "sp", combine, identity)
    combined = local_result + jnp.einsum(
        "zed,zdp->zep",
        recurrent_queries * jnp.exp(running_state),
        incoming_state,
        precision=lax.Precision.HIGHEST,
    )
    rec_heads = norm_rows(combined, recurrence_gain).astype(jnp.bfloat16)
    rec_rows = rec_heads.transpose(1, 0, 2).reshape(row_count, local_heads * DV)
    partial_value = jnp.dot(att_rows, att_out_weight, preferred_element_type=jnp.float32) + jnp.dot(
        rec_rows, rec_out_weight, preferred_element_type=jnp.float32
    )
    mixed_out = lax.psum(partial_value.astype(jnp.bfloat16), "tp")
    return (mixed_out, log_weight_sum)


def solution(mesh):
    return jax.shard_map(
        on_device,
        mesh=mesh,
        in_specs=(
            P(("fs", "sp"), None),
            P(),
            P(None, ("tp", "fs")),
            P(None, ("tp", "fs")),
            P(None, ("tp", "fs")),
            P(None, ("tp", "fs")),
            P(None, ("tp", "fs")),
            P(None, ("tp", "fs")),
            P("tp"),
            P("tp", None),
            P(("fs", "sp")),
            P(),
            P(),
            P("tp", None),
            P("tp", None),
        ),
        out_specs=(P(("fs", "sp"), None), P("tp", ("fs", "sp"))),
        check_vma=False,
    )
```

profile of v0, /device:TPU:0, one launch (start us, length us, event | category | flops | bytes accessed | tf_op | source)
XLA Modules:
  0.0 177.1 jit_solution(9279672745273595247)
XLA Ops:
  7.2 0.0 copy-start
  7.2 0.0 all-gather.4.cloned.1.call-start
  7.3 1.1 bitcast_dynamic-update-slice_fusion.5
  8.3 1.0 bitcast_dynamic-update-slice_fusion.4
  9.3 1.0 bitcast_dynamic-update-slice_fusion.3
  10.3 0.0 copy-start.2
  10.4 0.0 copy-start.8
  10.4 0.0 copy-start.7
  10.5 1.1 copy-done.1
  11.6 0.0 all-gather.4.cloned.1.call-update
  11.6 0.0 all-reduce.2.cloned.1.call-start
  11.7 0.2 fusion.46
  11.9 72.6 %all-gather.4.cloned.1.call-done = bf16[2048,6,256]{0,2,1:T(8,128)(2,1)} async-done(((bf16[2048,6,64]{0,2,1:T(8,128)(2,1)}), bf16[2048,6,256]{0,2,1:T(8,128)(2,1)}) %all-gather.4.cloned.1.call-update) | async-done | bytes 6291472 | tf_op jit(solution)/shard_map/all_gather | solution.py:156
  84.5 5.0 %convolution_convert_fusion = bf16[128,6,256]{2,0,1:T(8,128)(2,1)S(1)} fusion(bf16[2048,6,256]{0,2,1:T(8,128)(2,1)} %all-gather.4.cloned.1.call-done, bf16[128,2048]{1,0:T(8,128)(2,1)S(1)} %copy-done.2, f32[2048]{0:T(1024)S(1)} %copy-done.7, f32[128]{0:T(128)S(1)} %add_rsqrt_fusion.2), kind=kOutput, calls=%fused_computation.66 | convolution fusion | flops 806551552 | bytes 7217664 | tf_op jit(solution)/shard_map/rd,dnc->rnc/dot_general | solution.py:153
  89.6 0.0 copy-start.9
  89.6 0.1 copy.61
  89.8 0.1 copy.62
  89.9 0.3 fusion.75
  90.2 0.1 fusion.54
  90.3 3.4 %collective-permute-start = (bf16[1,2,128,256]{3,2,1,0:T(8,128)(2,1)S(1)}, bf16[1,2,128,256]{3,2,1,0:T(8,128)(2,1)S(1)}, u32[]{:S(2)}, u32[]{:S(2)}) collective-permute-start(bf16[1,2,128,256]{3,2,1,0:T(8,128)(2,1)S(1)} %maximum_bitcast_fusion), channel_id=1, source_target_pairs={{0,8},{8,16},{16,24},{1,9},{9,17},{17,25},{2,10},{10,18},{18,26},{... | collective-permute-start | bytes 393224 | tf_op jit(solution)/shard_map/ppermute | solution.py:16
  93.7 0.1 reshape.122
  93.8 0.1 reshape.123
  93.9 0.1 reshape.120
  94.0 0.1 exponential_subtract_fusion
  94.1 16.1 %while.52 = (s32[]{:T(128)}, f32[2,128,128]{2,1,0:T(8,128)S(1)}, f32[2,2,64,128]{3,2,0,1:T(8,128)S(1)}, f32[2,2,64,128]{3,2,0,1:T(8,128)S(1)}, f32[2,2,64,128]{3...) while((s32[]{:T(128)}, f32[2,128,128]{2,1,0:T(8,128)S(1)}, ...), condition=%wide.region_16.17_spmd.clone, body=%wide.region_14.16_spmd.clone.sunk | while | flops 79876096 | bytes 1818748 | solution.py:75
  94.1 0.1 reduce_window_sum.25
  94.3 7.0 %fusion.110 = f32[2,64,1,64]{3,2,1,0:T(1,128)S(1)} fusion(f32[2,64,128,1]{2,3,1,0:T(1,128)S(1)} %bitcast.210, f32[2,64,128]{2,1,0:T(8,128)S(1)} %get-tuple-element.685, f32[2,64,128]{2,1,0:T(8,128)S(1)} %reduce_window_sum.25, pred[64,64]{1,0:T(8,128)(4,1)S(1)} %iota_compare_fusion.3), kind=kOutput, calls=%fused_computation.22.clone.1 | convolution fusion | flops 15728640 | bytes 233472 | tf_op jit(solution)/shard_map/while/body/eval_jaxpr/htk,htsk,hsk->hts/dot_general | solution.py:59
  101.2 0.3 fusion.109
  101.5 0.2 fusion.111
  101.7 0.4 convolution_add_fusion.8
  102.2 0.1 reduce_window_sum.25
  102.3 7.0 %fusion.110 = f32[2,64,1,64]{3,2,1,0:T(1,128)S(1)} fusion(f32[2,64,128,1]{2,3,1,0:T(1,128)S(1)} %bitcast.210, f32[2,64,128]{2,1,0:T(8,128)S(1)} %get-tuple-element.685, f32[2,64,128]{2,1,0:T(8,128)S(1)} %reduce_window_sum.25, pred[64,64]{1,0:T(8,128)(4,1)S(1)} %iota_compare_fusion.3), kind=kOutput, calls=%fused_computation.22.clone.1 | convolution fusion | flops 15728640 | bytes 233472 | tf_op jit(solution)/shard_map/while/body/eval_jaxpr/htk,htsk,hsk->hts/dot_general | solution.py:59
  109.3 0.3 fusion.109
  109.5 0.2 fusion.111
  109.8 0.4 convolution_add_fusion.8
  110.2 15.5 %all-gather.1 = f32[8,128,128]{2,1,0:T(8,128)S(1)} all-gather(f32[2,128,128]{2,1,0:T(8,128)S(1)} %get-tuple-element.398), channel_id=3, replica_groups=mesh['sp'=4,'fs'=4,'tp'=2] {'sp'}, dimensions={0}, use_global_device_ids=true | all-gather | bytes 655360 | tf_op jit(solution)/shard_map/all_gather | solution.py:21
  125.7 0.2 reduce_window_sum.22
  125.9 8.8 %all-gather = f32[8,1,128]{2,1,0:T(1,128)S(1)} all-gather(f32[2,1,128]{2,1,0:T(1,128)S(1)} %slice_exponential_fusion), channel_id=2, replica_groups=mesh['sp'=4,'fs'=4,'tp'=2] {'sp'}, dimensions={0}, use_global_device_ids=true | all-gather | bytes 5120 | tf_op jit(solution)/shard_map/all_gather | solution.py:21
  134.7 0.5 while.53
  134.7 0.1 fusion.112
  134.9 0.1 fusion.112
  135.1 0.1 fusion.112
  135.2 0.1 copy.79
  135.3 0.4 multiply_reduce_fusion
  135.8 0.2 convolution_add_fusion.5
  136.1 1.6 collective-permute-start.1
  137.7 0.1 multiply_convert_fusion
  137.8 3.8 %collective-permute-done.1 = bf16[2,2,128,256]{3,2,1,0:T(8,128)(2,1)S(1)} collective-permute-done((bf16[2,2,128,256]{3,2,1,0:T(8,128)(2,1)S(1)}, bf16[2,2,128,256]{3,2,1,0:T(8,128)(2,1)S(1)}, u32[]{:S(2)}, u32[]{:S(2)}) %collective-permute-start.1) | collective-permute-done | bytes 262176 | tf_op jit(solution)/shard_map/ppermute | solution.py:16
  141.5 0.2 copy.66
  141.7 0.0 copy-start.11
  141.7 0.0 copy-start.12
  141.7 0.1 while.51
  141.9 0.0 copy-start.3
  141.9 0.1 copy.67
  142.0 0.4 copy-done.11
  142.4 0.1 multiply_reduce_fusion.1
  142.5 0.1 multiply_convert_fusion.1
  142.6 0.3 fusion.76
  142.9 0.1 copy-done.3
  143.1 1.1 fusion.44
  144.2 0.0 all-reduce.2.cloned.1.call-update
  144.2 0.6 fusion.67
  144.8 23.5 %all-reduce.2.cloned.1.call-done = bf16[128,2048]{1,0:T(8,128)(2,1)} async-done(((bf16[128,2048]{1,0:T(8,128)(2,1)}), bf16[128,2048]{1,0:T(8,128)(2,1)}) %all-reduce.2.cloned.1.call-update) | async-done | bytes 524304 | tf_op jit(solution)/shard_map/psum | solution.py:218
  168.3 1.9 %copy.167 = bf16[128,2048]{1,0:T(8,128)(2,1)} copy(bf16[128,2048]{1,0:T(8,128)(2,1)} %all-reduce.2.cloned.1.call-done) | data formatting | bytes 1048576
  (58 shorter events, 0.5 us)
Async XLA Ops:
  7.2 135.4 %copy-start = (bf16[256,2048]{1,0:T(8,128)(2,1)S(1)}, bf16[256,2048]{1,0:T(8,128)(2,1)}, u32[]{:S(2)}) copy-start(bf16[256,2048]{1,0:T(8,128)(2,1)} %param.38) | copy-start | bytes 3145732
  7.2 3.1 %copy-start.4 = (bf16[2048,64]{0,1:T(8,128)(2,1)S(1)}, bf16[2048,64]{0,1:T(8,128)(2,1)}, u32[]{:S(2)}) copy-start(bf16[2048,64]{0,1:T(8,128)(2,1)} %param.30) | copy-start | bytes 786436
  7.2 77.3 %all-gather.4.cloned.1.call-start = ((), (), s32[]{:S(2)}) async-start(), calls=%async_computation | async-start | bytes 7864320 | tf_op jit(solution)/shard_map/all_gather | solution.py:156
  7.2 3.1 %copy-start.5 = (bf16[2048,64]{0,1:T(8,128)(2,1)S(1)}, bf16[2048,64]{0,1:T(8,128)(2,1)}, u32[]{:S(2)}) copy-start(bf16[2048,64]{0,1:T(8,128)(2,1)} %param.31) | copy-start | bytes 786436
  7.2 3.2 %copy-start.6 = (bf16[2048,64]{0,1:T(8,128)(2,1)S(1)}, bf16[2048,64]{0,1:T(8,128)(2,1)}, u32[]{:S(2)}) copy-start(bf16[2048,64]{0,1:T(8,128)(2,1)} %param.32) | copy-start | bytes 786436
  10.3 1.4 copy-start.2
  10.4 1.6 copy-start.8
  10.4 74.2 %copy-start.7 = (f32[2048]{0:T(1024)S(1)}, f32[2048]{0:T(1024)}, u32[]{:S(2)}) copy-start(f32[2048]{0:T(1024)} %param.26) | copy-start | bytes 24580
  10.4 1.1 copy-start.1
  11.6 156.7 %all-reduce.2.cloned.1.call-start = ((), (), s32[]{:S(2)}) async-start(), calls=%async_computation.1 | async-start | bytes 1048576 | tf_op jit(solution)/shard_map/psum | solution.py:218
  89.6 4.4 %copy-start.9 = (f32[128]{0:T(128)S(1)}, f32[128]{0:T(128)}, u32[]{:S(2)}) copy-start(f32[128]{0:T(128)} %param.35) | copy-start | bytes 1540
  90.3 45.7 %collective-permute-start = (bf16[1,2,128,256]{3,2,1,0:T(8,128)(2,1)S(1)}, bf16[1,2,128,256]{3,2,1,0:T(8,128)(2,1)S(1)}, u32[]{:S(2)}, u32[]{:S(2)}) collective-permute-start(bf16[1,2,128,256]{3,2,1,0:T(8,128)(2,1)S(1)} %maximum_bitcast_fusion), channel_id=1, source_target_pairs={{0,8},{8,16},{16,24},{1,9},{9,17},{17,25},{2,10},{10,18},{18,26},{... | collective-permute-start | bytes 393224 | tf_op jit(solution)/shard_map/ppermute | solution.py:16
  134.7 2.9 %copy-start.10 = (f32[128]{0:T(128)S(1)}, f32[128]{0:T(128)}, u32[]{:S(2)}) copy-start(f32[128]{0:T(128)} %param.37) | copy-start | bytes 1540
  136.1 5.5 %collective-permute-start.1 = (bf16[2,2,128,256]{3,2,1,0:T(8,128)(2,1)S(1)}, bf16[2,2,128,256]{3,2,1,0:T(8,128)(2,1)S(1)}, u32[]{:S(2)}, u32[]{:S(2)}) collective-permute-start(bf16[2,2,128,256]{3,2,1,0:T(8,128)(2,1)S(1)} %pad_maximum_fusion), channel_id=1, source_target_pairs={{0,16},{8,24},{1,17},{9,25},{2,18},{10,26},{3,19},{11,27},{4,20},{... | collective-permute-start | bytes 786440 | tf_op jit(solution)/shard_map/ppermute | solution.py:16
  141.7 0.7 copy-start.11
  141.7 0.8 copy-start.12
  141.9 1.2 copy-start.3
Sparse Core Ops, SparseCore 0:
  11.7 72.7 all-gather.3
  144.4 23.9 all-reduce.1
where the time goes:
time: 177 us
  waiting for transfers between devices  99.9 us (56%)
  blocking collectives  24.4 us (14%)
  matrix products  23 us (13%)
  between operations  14.6 us (8%)
  local copies, waits for them, and re-layouts  7.66 us (4%)
  starting transfers between devices  5.05 us (3%)
  other arithmetic  2.18 us (1%)
    all_gather x1, waiting for transfers between devices, on_device(): lax.all_gather(stacked, 'fs', axis=2, tiled=True)  72.6 us
    all_gather x2, blocking collectives, entering(): pieces = jax.tree.map(lambda part: lax.all_gather(part, axis), value)  24.4 us
    psum x1, waiting for transfers between devices, on_device(): mixed_out = lax.psum(partial_value.astype(jnp.bfloat16), 'tp')  23.5 us
    dot_general x2, matrix products, advance(): jnp.einsum('htk,htsk,hsk->hts', query_block, decay, key_block, precision=...  13.9 us
    unnamed x32, local copies, waits for them, and re-layouts  6.65 us
    dot_general x1, matrix products, on_device(): jnp.einsum('rd,dnc->rnc', normed, lax.all_gather(stacked, 'fs', axis=2, t...  5 us
    ppermute x2, starting transfers between devices, from_behind(): lax.ppermute(value, axis, [(source, source + steps) for source in range(i...  4.97 us
    ppermute x2, waiting for transfers between devices, from_behind(): lax.ppermute(value, axis, [(source, source + steps) for source in range(i...  3.77 us
  transfers between devices with their start and end apart: 4, of which 3 were waited for; matrix products, arithmetic and copies ran while one was open for 10% of the time, Pallas kernels for 0%

commit v1 on v0

--- a/solution.py
+++ b/solution.py
@@ -215,7 +215,9 @@
     partial_value = jnp.dot(att_rows, att_out_weight, preferred_element_type=jnp.float32) + jnp.dot(
         rec_rows, rec_out_weight, preferred_element_type=jnp.float32
     )
-    mixed_out = lax.psum(partial_value.astype(jnp.bfloat16), "tp")
+    own = partial_value.astype(jnp.bfloat16)
+    parts = lax.all_gather(own, "tp", axis=0, tiled=False)
+    mixed_out = parts.sum(axis=0)
     return (mixed_out, log_weight_sum)
 
 

time: 177 us -> 168 us (0.949)
  waiting for transfers between devices: 99.9 us -> 90.3 us
  other arithmetic: 2.18 us -> 4.54 us
  local copies, waits for them, and re-layouts: 7.66 us -> 5.78 us
    psum x1 -> x0, waiting for transfers between devices: 23.5 us -> none  [on_device(): mixed_out = lax.psum(partial_value.astype(jnp.bfloat16), 'tp')]
    all_gather x0 -> x1, waiting for transfers between devices: none -> 13.9 us  [on_device(): parts = lax.all_gather(own, 'tp', axis=0, tiled=False)]
    reduce_sum x0 -> x1, other arithmetic: none -> 2.36 us  [on_device(): mixed_out = parts.sum(axis=0)]
    unnamed x32 -> x33, local copies, waits for them, and re-layouts: 6.65 us -> 4.77 us
  transfers between devices with their start and end apart: 4 -> 4, of which waited for: 3 -> 3; matrix products, arithmetic and copies ran while one was open for 10% -> 11% of each run, Pallas kernels for 0% -> 0%
where the time goes in v1:
time: 168 us
  waiting for transfers between devices  90.3 us (54%)
  blocking collectives  24.3 us (14%)
  matrix products  23 us (14%)
  between operations  14.6 us (9%)
  local copies, waits for them, and re-layouts  5.78 us (3%)
  starting transfers between devices  5.05 us (3%)
  other arithmetic  4.54 us (3%)
    all_gather x1, waiting for transfers between devices, on_device(): lax.all_gather(stacked, 'fs', axis=2, tiled=True)  72.6 us
    all_gather x2, blocking collectives, entering(): pieces = jax.tree.map(lambda part: lax.all_gather(part, axis), value)  24.3 us
    all_gather x1, waiting for transfers between devices, on_device(): parts = lax.all_gather(own, 'tp', axis=0, tiled=False)  13.9 us
    dot_general x2, matrix products, advance(): jnp.einsum('htk,htsk,hsk->hts', query_block, decay, key_block, precision=...  13.9 us
    dot_general x1, matrix products, on_device(): jnp.einsum('rd,dnc->rnc', normed, lax.all_gather(stacked, 'fs', axis=2, t...  5 us
    ppermute x2, starting transfers between devices, from_behind(): lax.ppermute(value, axis, [(source, source + steps) for source in range(i...  4.97 us
    unnamed x33, local copies, waits for them, and re-layouts  4.77 us
    ppermute x2, waiting for transfers between devices, from_behind(): lax.ppermute(value, axis, [(source, source + steps) for source in range(i...  3.77 us
  transfers between devices with their start and end apart: 4, of which 3 were waited for; matrix products, arithmetic and copies ran while one was open for 11% of the time, Pallas kernels for 0%

profile of v1, /device:TPU:0, one launch (start us, length us, event | category | flops | bytes accessed | tf_op | source)
XLA Modules:
  0.0 167.9 jit_solution(11043881477849688961)
XLA Ops:
  7.2 0.0 copy-start
  7.2 0.0 all-gather.6.cloned.1.call-start
  7.3 1.1 bitcast_dynamic-update-slice_fusion.5
  8.3 1.0 bitcast_dynamic-update-slice_fusion.4
  9.3 1.0 bitcast_dynamic-update-slice_fusion.3
  10.3 0.0 copy-start.2
  10.4 0.0 copy-start.9
  10.4 0.0 copy-start.8
  10.5 1.1 copy-done.1
  11.6 0.0 all-gather.6.cloned.1.call-update
  11.6 0.0 all-gather.8.cloned.1.call-start
  11.7 0.2 fusion.46
  11.9 72.6 %all-gather.6.cloned.1.call-done = bf16[2048,6,256]{0,2,1:T(8,128)(2,1)} async-done(((bf16[2048,6,64]{0,2,1:T(8,128)(2,1)}), bf16[2048,6,256]{0,2,1:T(8,128)(2,1)}) %all-gather.6.cloned.1.call-update) | async-done | bytes 6291472 | tf_op jit(solution)/shard_map/all_gather | solution.py:156
  84.5 5.0 %convolution_convert_fusion = bf16[128,6,256]{2,0,1:T(8,128)(2,1)S(1)} fusion(bf16[2048,6,256]{0,2,1:T(8,128)(2,1)} %all-gather.6.cloned.1.call-done, bf16[128,2048]{1,0:T(8,128)(2,1)S(1)} %copy-done.2, f32[2048]{0:T(1024)S(1)} %copy-done.8, f32[128]{0:T(128)S(1)} %add_rsqrt_fusion.2), kind=kOutput, calls=%fused_computation.66 | convolution fusion | flops 806551552 | bytes 7217664 | tf_op jit(solution)/shard_map/rd,dnc->rnc/dot_general | solution.py:153
  89.6 0.0 copy-start.10
  89.6 0.1 copy.61
  89.7 0.1 copy.62
  89.9 0.0 copy-start.7
  89.9 0.3 fusion.75
  90.2 0.1 fusion.54
  90.3 3.4 %collective-permute-start = (bf16[1,2,128,256]{3,2,1,0:T(8,128)(2,1)S(1)}, bf16[1,2,128,256]{3,2,1,0:T(8,128)(2,1)S(1)}, u32[]{:S(2)}, u32[]{:S(2)}) collective-permute-start(bf16[1,2,128,256]{3,2,1,0:T(8,128)(2,1)S(1)} %maximum_bitcast_fusion), channel_id=1, source_target_pairs={{0,8},{8,16},{16,24},{1,9},{9,17},{17,25},{2,10},{10,18},{18,26},{... | collective-permute-start | bytes 393224 | tf_op jit(solution)/shard_map/ppermute | solution.py:16
  93.7 0.1 reshape.122
  93.8 0.1 reshape.123
  93.9 0.1 reshape.120
  94.0 0.1 exponential_subtract_fusion
  94.1 16.1 %while.52 = (s32[]{:T(128)}, f32[2,128,128]{2,1,0:T(8,128)S(1)}, f32[2,2,64,128]{3,2,0,1:T(8,128)S(1)}, f32[2,2,64,128]{3,2,0,1:T(8,128)S(1)}, f32[2,2,64,128]{3...) while((s32[]{:T(128)}, f32[2,128,128]{2,1,0:T(8,128)S(1)}, ...), condition=%wide.region_16.17_spmd.clone, body=%wide.region_14.16_spmd.clone.sunk | while | flops 79876096 | bytes 1818748 | solution.py:75
  94.1 0.1 reduce_window_sum.25
  94.3 6.9 %fusion.110 = f32[2,64,1,64]{3,2,1,0:T(1,128)S(1)} fusion(f32[2,64,128,1]{2,3,1,0:T(1,128)S(1)} %bitcast.211, f32[2,64,128]{2,1,0:T(8,128)S(1)} %get-tuple-element.685, f32[2,64,128]{2,1,0:T(8,128)S(1)} %reduce_window_sum.25, pred[64,64]{1,0:T(8,128)(4,1)S(1)} %iota_compare_fusion.3), kind=kOutput, calls=%fused_computation.22.clone.1 | convolution fusion | flops 15728640 | bytes 233472 | tf_op jit(solution)/shard_map/while/body/eval_jaxpr/htk,htsk,hsk->hts/dot_general | solution.py:59
  101.2 0.3 fusion.109
  101.5 0.2 fusion.111
  101.7 0.4 convolution_add_fusion.8
  102.2 0.1 reduce_window_sum.25
  102.3 6.9 %fusion.110 = f32[2,64,1,64]{3,2,1,0:T(1,128)S(1)} fusion(f32[2,64,128,1]{2,3,1,0:T(1,128)S(1)} %bitcast.211, f32[2,64,128]{2,1,0:T(8,128)S(1)} %get-tuple-element.685, f32[2,64,128]{2,1,0:T(8,128)S(1)} %reduce_window_sum.25, pred[64,64]{1,0:T(8,128)(4,1)S(1)} %iota_compare_fusion.3), kind=kOutput, calls=%fused_computation.22.clone.1 | convolution fusion | flops 15728640 | bytes 233472 | tf_op jit(solution)/shard_map/while/body/eval_jaxpr/htk,htsk,hsk->hts/dot_general | solution.py:59
  109.2 0.3 fusion.109
  109.5 0.2 fusion.111
  109.7 0.4 convolution_add_fusion.8
  110.2 15.5 %all-gather.1 = f32[8,128,128]{2,1,0:T(8,128)S(1)} all-gather(f32[2,128,128]{2,1,0:T(8,128)S(1)} %get-tuple-element.398), channel_id=3, replica_groups=mesh['sp'=4,'fs'=4,'tp'=2] {'sp'}, dimensions={0}, use_global_device_ids=true | all-gather | bytes 655360 | tf_op jit(solution)/shard_map/all_gather | solution.py:21
  125.7 0.2 reduce_window_sum.22
  125.9 8.8 %all-gather = f32[8,1,128]{2,1,0:T(1,128)S(1)} all-gather(f32[2,1,128]{2,1,0:T(1,128)S(1)} %slice_exponential_fusion), channel_id=2, replica_groups=mesh['sp'=4,'fs'=4,'tp'=2] {'sp'}, dimensions={0}, use_global_device_ids=true | all-gather | bytes 5120 | tf_op jit(solution)/shard_map/all_gather | solution.py:21
  134.7 0.5 while.53
  134.7 0.1 fusion.112
  134.9 0.1 fusion.112
  135.0 0.1 fusion.112
  135.2 0.1 copy.79
  135.3 0.4 multiply_reduce_fusion
  135.7 0.2 convolution_add_fusion.5
  136.0 1.6 collective-permute-start.1
  137.6 0.1 multiply_convert_fusion
  137.7 3.8 %collective-permute-done.1 = bf16[2,2,128,256]{3,2,1,0:T(8,128)(2,1)S(1)} collective-permute-done((bf16[2,2,128,256]{3,2,1,0:T(8,128)(2,1)S(1)}, bf16[2,2,128,256]{3,2,1,0:T(8,128)(2,1)S(1)}, u32[]{:S(2)}, u32[]{:S(2)}) %collective-permute-start.1) | collective-permute-done | bytes 262176 | tf_op jit(solution)/shard_map/ppermute | solution.py:16
  141.5 0.2 copy.66
  141.7 0.0 copy-start.13
  141.7 0.1 while.51
  141.8 0.0 copy-start.3
  141.8 0.1 copy.67
  142.0 0.4 copy-done.12
  142.3 0.1 multiply_reduce_fusion.1
  142.4 0.1 multiply_convert_fusion.1
  142.6 0.3 fusion.76
  142.9 0.1 copy-done.3
  143.0 1.1 fusion.44
  144.2 0.0 all-gather.8.cloned.1.call-update
  144.2 0.6 fusion.67
  144.8 13.9 %all-gather.8.cloned.1.call-done = bf16[256,2048]{1,0:T(8,128)(2,1)} async-done(((bf16[128,2048]{1,0:T(8,128)(2,1)}), bf16[256,2048]{1,0:T(8,128)(2,1)}) %all-gather.8.cloned.1.call-update) | async-done | bytes 1048592 | tf_op jit(solution)/shard_map/all_gather | solution.py:219
  158.7 2.4 %reduce_sum.72 = bf16[128,2048]{1,0:T(8,128)(2,1)} reduce(bf16[2,128,2048]{2,1,0:T(8,128)(2,1)} %bitcast.224, bf16[]{:T(256)} %constant.144.clone.1), dimensions={0}, to_apply=%region_21.22 | reduce | flops 262144 | bytes 1572866 | tf_op jit(solution)/shard_map/reduce_sum | solution.py:220
  (60 shorter events, 0.5 us)
Async XLA Ops:
  7.2 135.4 %copy-start = (bf16[256,2048]{1,0:T(8,128)(2,1)S(1)}, bf16[256,2048]{1,0:T(8,128)(2,1)}, u32[]{:S(2)}) copy-start(bf16[256,2048]{1,0:T(8,128)(2,1)} %param.38) | copy-start | bytes 3145732
  7.2 3.1 %copy-start.4 = (bf16[2048,64]{0,1:T(8,128)(2,1)S(1)}, bf16[2048,64]{0,1:T(8,128)(2,1)}, u32[]{:S(2)}) copy-start(bf16[2048,64]{0,1:T(8,128)(2,1)} %param.30) | copy-start | bytes 786436
  7.2 77.3 %all-gather.6.cloned.1.call-start = ((), (), s32[]{:S(2)}) async-start(), calls=%async_computation | async-start | bytes 7864320 | tf_op jit(solution)/shard_map/all_gather | solution.py:156
  7.2 3.1 %copy-start.5 = (bf16[2048,64]{0,1:T(8,128)(2,1)S(1)}, bf16[2048,64]{0,1:T(8,128)(2,1)}, u32[]{:S(2)}) copy-start(bf16[2048,64]{0,1:T(8,128)(2,1)} %param.31) | copy-start | bytes 786436
  7.2 3.2 %copy-start.6 = (bf16[2048,64]{0,1:T(8,128)(2,1)S(1)}, bf16[2048,64]{0,1:T(8,128)(2,1)}, u32[]{:S(2)}) copy-start(bf16[2048,64]{0,1:T(8,128)(2,1)} %param.32) | copy-start | bytes 786436
  10.3 1.4 copy-start.2
  10.4 1.6 copy-start.9
  10.4 74.1 %copy-start.8 = (f32[2048]{0:T(1024)S(1)}, f32[2048]{0:T(1024)}, u32[]{:S(2)}) copy-start(f32[2048]{0:T(1024)} %param.26) | copy-start | bytes 24580
  10.4 1.1 copy-start.1
  11.6 147.1 %all-gather.8.cloned.1.call-start = ((), (), s32[]{:S(2)}) async-start(), calls=%async_computation.1 | async-start | bytes 1572864 | tf_op jit(solution)/shard_map/all_gather | solution.py:219
  89.6 4.4 %copy-start.10 = (f32[128]{0:T(128)S(1)}, f32[128]{0:T(128)}, u32[]{:S(2)}) copy-start(f32[128]{0:T(128)} %param.35) | copy-start | bytes 1540
  89.9 4.2 %copy-start.7 = (f32[2,2,64,128]{3,2,0,1:T(8,128)S(1)}, f32[2,2,64,128]{3,2,0,1:T(8,128)}, u32[]{:S(2)}) copy-start(f32[2,2,64,128]{3,2,0,1:T(8,128)} %custom-call.3) | copy-start | bytes 393220
  90.3 45.7 %collective-permute-start = (bf16[1,2,128,256]{3,2,1,0:T(8,128)(2,1)S(1)}, bf16[1,2,128,256]{3,2,1,0:T(8,128)(2,1)S(1)}, u32[]{:S(2)}, u32[]{:S(2)}) collective-permute-start(bf16[1,2,128,256]{3,2,1,0:T(8,128)(2,1)S(1)} %maximum_bitcast_fusion), channel_id=1, source_target_pairs={{0,8},{8,16},{16,24},{1,9},{9,17},{17,25},{2,10},{10,18},{18,26},{... | collective-permute-start | bytes 393224 | tf_op jit(solution)/shard_map/ppermute | solution.py:16
  134.7 2.9 %copy-start.11 = (f32[128]{0:T(128)S(1)}, f32[128]{0:T(128)}, u32[]{:S(2)}) copy-start(f32[128]{0:T(128)} %param.37) | copy-start | bytes 1540
  136.0 5.5 %collective-permute-start.1 = (bf16[2,2,128,256]{3,2,1,0:T(8,128)(2,1)S(1)}, bf16[2,2,128,256]{3,2,1,0:T(8,128)(2,1)S(1)}, u32[]{:S(2)}, u32[]{:S(2)}) collective-permute-start(bf16[2,2,128,256]{3,2,1,0:T(8,128)(2,1)S(1)} %pad_maximum_fusion), channel_id=1, source_target_pairs={{0,16},{8,24},{1,17},{9,25},{2,18},{10,26},{3,19},{11,27},{4,20},{... | collective-permute-start | bytes 786440 | tf_op jit(solution)/shard_map/ppermute | solution.py:16
  141.7 0.7 copy-start.12
  141.7 0.8 copy-start.13
  141.8 1.2 copy-start.3
Sparse Core Ops, SparseCore 0:
  11.7 72.7 all-gather.5
  144.3 14.3 all-gather.7
